TPU v7x, 32 devices: a whole 2x2x4 slice. The times are simulated.
32 devices in a mesh: kv: 16 (over z, x, core), tp: 2 (over y).
Axes of the slice: x: 2, y: 2, z: 4, core: 2. Of those that a mesh axis runs over, the one named last changes fastest.
Arguments:
- queries: bfloat16 [2048, 4096], P('kv', 'tp'), may hold values from -6 to 6
- keys: bfloat16 [2048, 512], P('kv', 'tp'), may hold values from -6 to 6
- values: bfloat16 [2048, 512], P('kv', 'tp'), may hold values from -6 to 6
- logsum: float32 [2048, 32], P('kv', 'tp'), may hold values from 2 to 6
- out_grad: bfloat16 [2048, 4096], P('kv', 'tp'), may hold values from -6 to 6
- normed_input: bfloat16 [2048, 4096], P('kv', 'tp'), may hold values from -6 to 6
- chosen: int32 [32, 16], P('kv'), may hold values from 0 to 63, as said below
Outputs:
- query_grad: float32 [2048, 4096], P('kv', 'tp')
- key_grad: float32 [2048, 512], P('kv', 'tp')
- value_grad: float32 [2048, 512], P('kv', 'tp')
- value_weight_grad: float32 [4096, 512], P('kv', 'tp')
Inputs may be any that keep to these rules, and one draw needn't show every extreme that they name: `chosen`: each row r names 16 distinct key blocks, among them block 0 and the blocks r * 2 to r * 2 + 64 / 32 - 1 that hold the query block's own positions. The rows of one device (aligned runs of 2 rows) name at most one block of any other device's 128 / 32 blocks. Blocks after the query block may be named; their keys are masked.
All inputs are finite; a program needn't handle non-finite values.
Results may differ from a plain program's by a relative error of at most 0.008.
Values may be sent and summed in bfloat16 or wider, within the bound.
A program may use at most 64 MiB of HBM per device.

v0:
```python
import jax
import jax.numpy as jnp
from jax import lax
from jax.sharding import PartitionSpec as P

HD = 128
QB = 64
KB = 32
NSEL = 16


def local(queries, keys, values, logsum, out_grad, normed_input, chosen):
    devices = lax.axis_size("kv")
    here = lax.axis_index("kv")
    tok = keys.shape[0]
    kv_cols = keys.shape[1]
    kv_heads = kv_cols // HD
    group = queries.shape[1] // kv_cols
    kblocks = tok // KB
    qblocks = tok // QB
    span = NSEL * KB
    scale = HD ** (-0.5)
    owner = chosen // kblocks
    within = chosen % kblocks
    remote = owner != here
    peers = jnp.arange(devices, dtype=jnp.int32)
    named = (owner[:, :, None] == peers[None, None, :]) & remote[:, :, None]
    wanted = jnp.max(jnp.where(named, within[:, :, None] + 1, 0), axis=(0, 1))
    asked = (
        lax.all_to_all(
            wanted.reshape(devices, 1), "kv", split_axis=0, concat_axis=0, tiled=True
        ).reshape(devices)
        - 1
    )
    key_blocks = keys.reshape(kblocks, KB, kv_cols)
    value_blocks = values.reshape(kblocks, KB, kv_cols)
    taken = jnp.maximum(asked, 0)
    live = (asked >= 0)[:, None, None]
    send_keys = jnp.where(live, key_blocks[taken], jnp.zeros((), keys.dtype))
    send_values = jnp.where(live, value_blocks[taken], jnp.zeros((), values.dtype))
    got_keys, got_values = (
        lax.all_to_all(send_keys, "kv", split_axis=0, concat_axis=0, tiled=True),
        lax.all_to_all(send_values, "kv", split_axis=0, concat_axis=0, tiled=True),
    )
    pool_keys = jnp.concatenate([key_blocks, got_keys], axis=0)
    pool_values = jnp.concatenate([value_blocks, got_values], axis=0)
    slot = jnp.where(remote, kblocks + owner, within)
    sel_keys = pool_keys[slot].reshape(qblocks, span, kv_heads, HD)
    sel_values = pool_values[slot].reshape(qblocks, span, kv_heads, HD)
    query_rows = queries.reshape(qblocks, QB, kv_heads, group, HD)
    dout = out_grad.reshape(qblocks, QB, kv_heads, group, HD)
    lse = logsum.reshape(qblocks, QB, kv_heads, group)
    scores = (
        jnp.einsum("bqngd,bjnd->bqngj", query_rows, sel_keys, preferred_element_type=jnp.float32)
        * scale
    )
    qpos = here * tok + jnp.arange(tok, dtype=jnp.int32).reshape(qblocks, QB)
    kpos = (chosen[:, :, None] * KB + jnp.arange(KB, dtype=jnp.int32)[None, None, :]).reshape(
        qblocks, span
    )
    valid = (kpos[:, None, :] <= qpos[:, :, None])[:, :, None, None, :]
    prob = jnp.where(valid, jnp.exp(scores - lse[..., None]), 0.0)
    dprob = jnp.einsum("bqngd,bjnd->bqngj", dout, sel_values, preferred_element_type=jnp.float32)
    delta = jnp.sum(prob * dprob, axis=-1, keepdims=True)
    dscore = (prob * (dprob - delta)).astype(jnp.bfloat16)
    prob_low = prob.astype(jnp.bfloat16)
    query_grad = (
        jnp.einsum("bqngj,bjnd->bqngd", dscore, sel_keys, preferred_element_type=jnp.float32)
        * scale
    )
    query_grad = query_grad.reshape(tok, queries.shape[1])
    key_part = (
        jnp.einsum("bqngj,bqngd->bjnd", dscore, query_rows, preferred_element_type=jnp.float32)
        * scale
    )
    value_part = jnp.einsum("bqngj,bqngd->bjnd", prob_low, dout, preferred_element_type=jnp.float32)
    entries = qblocks * NSEL
    pool_size = kblocks + devices
    onehot = (slot.reshape(entries, 1) == jnp.arange(pool_size, dtype=jnp.int32)[None, :]).astype(
        jnp.float32
    )
    key_sum = jnp.dot(
        onehot.T,
        key_part.reshape(entries, KB * kv_cols),
        precision=lax.Precision.HIGHEST,
        preferred_element_type=jnp.float32,
    )
    value_sum = jnp.dot(
        onehot.T,
        value_part.reshape(entries, KB * kv_cols),
        precision=lax.Precision.HIGHEST,
        preferred_element_type=jnp.float32,
    )
    back_keys = key_sum[kblocks:].reshape(devices, KB, kv_cols)
    back_values = value_sum[kblocks:].reshape(devices, KB, kv_cols)
    ret_keys, ret_values = (
        lax.all_to_all(back_keys, "kv", split_axis=0, concat_axis=0, tiled=True),
        lax.all_to_all(back_values, "kv", split_axis=0, concat_axis=0, tiled=True),
    )
    home = (asked[:, None] == jnp.arange(kblocks, dtype=jnp.int32)[None, :]).astype(jnp.float32)
    key_grad = key_sum[:kblocks] + jnp.dot(
        home.T,
        ret_keys.reshape(devices, KB * kv_cols),
        precision=lax.Precision.HIGHEST,
        preferred_element_type=jnp.float32,
    )
    value_grad = value_sum[:kblocks] + jnp.dot(
        home.T,
        ret_values.reshape(devices, KB * kv_cols),
        precision=lax.Precision.HIGHEST,
        preferred_element_type=jnp.float32,
    )
    key_grad = key_grad.reshape(tok, kv_cols)
    value_grad = value_grad.reshape(tok, kv_cols)
    value_low = value_grad.astype(jnp.bfloat16)
    full_input = lax.all_gather(normed_input, "tp", axis=1, tiled=True)
    weight_grad = lax.psum_scatter(
        jnp.einsum("td,tc->dc", full_input, value_low, preferred_element_type=jnp.float32),
        "kv",
        scatter_dimension=0,
        tiled=True,
    )
    return (query_grad, key_grad, value_grad, weight_grad)


def solution(mesh):
    in_specs = (
        P("kv", "tp"),
        P("kv", "tp"),
        P("kv", "tp"),
        P("kv", "tp"),
        P("kv", "tp"),
        P("kv", "tp"),
        P("kv", None),
    )
    out_specs = (P("kv", "tp"), P("kv", "tp"), P("kv", "tp"), P("kv", "tp"))
    return jax.shard_map(local, mesh=mesh, in_specs=in_specs, out_specs=out_specs, check_vma=False)
```

profile of v0, /device:TPU:0, one launch (start us, length us, event | category | flops | bytes accessed | tf_op | source)
XLA Modules:
  0.0 171.1 jit_solution(7793433736477169849)
XLA Ops:
  7.2 0.0 copy-start.4
  7.2 0.8 compare_select_fusion
  8.0 0.1 select_reduce_fusion
  8.1 0.7 copy.55
  8.7 7.4 %all-to-all-start = ((s32[16,1,1]{2,1,0:T(1,128)}), s32[16,1,1]{2,1,0:T(1,128)S(1)}, u32[]{:S(2)}, u32[]{:S(2)}) async-start(s32[16,1,1]{2,1,0:T(1,128)} %copy.55), calls=%async_computation | async-start | bytes 16384 | tf_op jit(solution)/shard_map/all_to_all | solution.py:30
  16.1 0.1 reshape.149
  16.2 6.3 %all-to-all-done = s32[16,1,1]{2,1,0:T(1,128)S(1)} async-done(((s32[16,1,1]{2,1,0:T(1,128)}), s32[16,1,1]{2,1,0:T(1,128)S(1)}, u32[]{:S(2)}, u32[]{:S(2)}) %all-to-all-start) | async-done | bytes 96 | tf_op jit(solution)/shard_map/all_to_all | solution.py:30
  22.5 0.7 fusion.35
  23.2 1.4 gather_fusion.2
  24.6 1.4 gather_fusion
  26.0 0.4 compare_reduce_fusion
  26.4 0.8 broadcast_select_fusion.1
  27.2 3.5 %all-to-all-start.1 = ((bf16[16,32,256]{2,1,0:T(8,128)(2,1)}), bf16[16,32,256]{2,1,0:T(8,128)(2,1)S(1)}, u32[]{:S(2)}, u32[]{:S(2)}) async-start(bf16[16,32,256]{2,1,0:T(8,128)(2,1)} %get-tuple-element.31), calls=%async_computation.1 | async-start | bytes 524288 | tf_op jit(solution)/shard_map/all_to_all | solution.py:42
  30.8 0.1 eq.46
  30.8 0.1 add.89
  30.9 0.1 add.86
  31.0 0.1 add.87
  31.1 0.8 sub.31
  31.9 1.1 copy.79
  33.0 0.1 copy.80
  33.1 0.0 copy-start.2
  33.2 0.1 broadcast_compare_fusion
  33.3 7.4 %all-to-all-done.1 = bf16[16,32,256]{2,1,0:T(8,128)(2,1)S(1)} async-done(((bf16[16,32,256]{2,1,0:T(8,128)(2,1)}), bf16[16,32,256]{2,1,0:T(8,128)(2,1)S(1)}, u32[]{:S(2)}, u32[]{:S(2)}) %all-to-all-start.1) | async-done | bytes 262176 | tf_op jit(solution)/shard_map/all_to_all | solution.py:42
  40.8 0.6 gather_fusion.1
  41.3 0.1 reshape.122
  41.5 0.7 fusion.20
  42.2 2.0 %copy-done = f32[2,2,512,64,8]{2,3,4,1,0:T(8,128)} copy-done((f32[2,2,512,64,8]{2,3,4,1,0:T(8,128)}, f32[2,2,512,64,8]{2,3,4,1,0:T(8,128)S(1)}, u32[]{:S(2)}) %copy-start) | copy-done | bytes 4194328
  44.2 1.8 %fusion.14 = f32[2,512,2,128]{3,1,2,0:T(8,128)S(1)} fusion(f32[2,2,512,64,8]{2,3,4,1,0:T(8,128)S(1)} %fusion.20, f32[2,64,2,8]{1,3,2,0:T(8,128)S(1)} %copy.58, pred[2,64,512]{2,1,0:T(8,128)(4,1)S(1)} %broadcast_compare_fusion, bf16[2,64,2,8,128]{4,3,2,1,0:T(8,128)(2,1)S(1)} %bitcast.77), kind=kOutput, calls=%fused_computation.24 | convolution fusion | flops 272629760 | bytes 5840896 | tf_op jit(solution)/shard_map/bqngj,bqngd->bjnd/dot_general | solution.py:76
  46.0 0.8 copy.66
  46.8 0.8 reshape.135
  47.6 0.6 fusion.28
  48.3 1.0 copy.83
  49.3 3.6 %all-to-all-start.4 = ((f32[16,32,256]{2,1,0:T(8,128)}), f32[16,32,256]{2,1,0:T(8,128)S(1)}, u32[]{:S(2)}, u32[]{:S(2)}) async-start(f32[16,32,256]{2,1,0:T(8,128)} %bitcast.30), calls=%async_computation.4 | async-start | bytes 1048576 | tf_op jit(solution)/shard_map/all_to_all | solution.py:98
  52.8 0.0 all-gather.2.cloned.1.call-start
  52.9 0.7 all-gather.2.cloned.1.call-update
  53.6 0.0 reduce-scatter.2.cloned.1.call-start
  53.6 13.5 %all-to-all-done.4 = f32[16,32,256]{2,1,0:T(8,128)S(1)} async-done(((f32[16,32,256]{2,1,0:T(8,128)}), f32[16,32,256]{2,1,0:T(8,128)S(1)}, u32[]{:S(2)}, u32[]{:S(2)}) %all-to-all-start.4) | async-done | bytes 524320 | tf_op jit(solution)/shard_map/all_to_all | solution.py:98
  67.1 0.3 copy.84
  67.4 0.4 convolution_add_fusion
  67.8 0.1 reshape.138
  67.9 9.9 %all-gather.2.cloned.1.call-done = bf16[128,4096]{1,0:T(8,128)(2,1)} async-done(((bf16[128,2048]{1,0:T(8,128)(2,1)}), bf16[128,4096]{1,0:T(8,128)(2,1)}) %all-gather.2.cloned.1.call-update) | async-done | bytes 1048592 | tf_op jit(solution)/shard_map/all_gather | solution.py:116
  77.8 3.9 %convolution_bitcast_fusion = f32[4096,256]{0,1:T(8,128)} fusion(bf16[128,4096]{1,0:T(8,128)(2,1)} %all-gather.2.cloned.1.call-done, f32[128,256]{1,0:T(8,128)S(1)} %reshape.138), kind=kOutput, calls=%fused_computation.6 | convolution fusion | flops 268468224 | bytes 5373952 | tf_op jit(solution)/shard_map/td,tc->dc/dot_general | solution.py:118
  81.7 0.0 reduce-scatter.2.cloned.1.call-update
  81.7 15.6 %all_to_all.29 = bf16[16,32,256]{2,1,0:T(8,128)(2,1)S(1)} all-to-all(bf16[16,32,256]{2,1,0:T(8,128)(2,1)S(1)} %get-tuple-element.32), channel_id=1, replica_groups=mesh['kv'=16,'tp'=2] {'kv'}, dimensions={0} | all-to-all | bytes 524288 | tf_op jit(solution)/shard_map/all_to_all | solution.py:43
  97.3 0.6 gather_fusion.3
  97.9 0.1 reshape.128
  98.1 3.6 %fusion = (f32[2,64,2,8]{1,3,2,0:T(8,128)S(1)}, f32[2,2,512,64,8]{2,3,4,1,0:T(8,128)S(1)}) fusion(f32[2,2,512,64,8]{2,3,4,1,0:T(8,128)} %copy-done, f32[2,64,2,8]{1,3,2,0:T(8,128)S(1)} %copy.58, pred[2,64,512]{2,1,0:T(8,128)(4,1)S(1)} %broadcast_compare_fusion, bf16[2,64,2,8,128]{4,3,2,1,0:T(8,128)(2,1)S(1)} %bitcast.78, ...), kind=kOutput, calls=%fused_computation.9 | convolution fusion | flops 273676288 | bytes 9519104 | tf_op jit(solution)/shard_map/bqngd,bjnd->bqngj/dot_general | solution.py:63
  101.7 0.3 copy-done.1
  101.9 1.5 fusion.2
  103.5 0.9 fusion.13
  104.4 1.8 %copy.64 = f32[2,512,2,128]{3,2,1,0:T(2,128)} copy(f32[2,512,2,128]{3,1,2,0:T(8,128)S(1)} %fusion.13) | data formatting | bytes 2097152 | tf_op jit(solution)/shard_map/mul | solution.py:73
  106.2 3.0 %reshape.131 = f32[32,8192]{1,0:T(8,128)} reshape(f32[2,512,2,128]{3,2,1,0:T(2,128)} %copy.64) | data formatting | bytes 2097152 | tf_op jit(solution)/shard_map/reshape | solution.py:84
  109.2 1.8 %fusion.29 = f32[20,8192]{1,0:T(8,128)S(1)} fusion(f32[32,8192]{1,0:T(8,128)} %reshape.131, s32[32]{0:T(128)S(1)} %eq.46), kind=kOutput, calls=%fused_computation.45 | convolution fusion | flops 62915200 | bytes 1704064 | tf_op jit(solution)/shard_map/dot_general | solution.py:82
  111.1 1.0 copy.81
  112.0 4.2 %all-to-all-start.3 = ((f32[16,32,256]{2,1,0:T(8,128)}), f32[16,32,256]{2,1,0:T(8,128)}, u32[]{:S(2)}, u32[]{:S(2)}) async-start(f32[16,32,256]{2,1,0:T(8,128)} %bitcast.81), calls=%async_computation.3 | async-start | bytes 1048576 | tf_op jit(solution)/shard_map/all_to_all | solution.py:97
  116.3 0.7 fusion.17
  117.0 0.6 copy.62
  117.6 1.1 reshape.130
  118.8 17.0 %all-to-all-done.3 = f32[16,32,256]{2,1,0:T(8,128)} async-done(((f32[16,32,256]{2,1,0:T(8,128)}), f32[16,32,256]{2,1,0:T(8,128)}, u32[]{:S(2)}, u32[]{:S(2)}) %all-to-all-start.3) | async-done | bytes 524320 | tf_op jit(solution)/shard_map/all_to_all | solution.py:97
  135.8 1.4 copy.82
  137.1 0.4 convolution_add_fusion.1
  137.5 0.7 reshape.134
  138.3 24.2 %reduce-scatter.2.cloned.1.call-done = f32[256,256]{0,1:T(8,128)} async-done(((f32[4096,256]{0,1:T(8,128)}), f32[256,256]{0,1:T(8,128)}) %reduce-scatter.2.cloned.1.call-update) | async-done | bytes 262160 | tf_op jit(solution)/shard_map/reduce_scatter | solution.py:117
  162.4 1.8 %copy.67 = f32[256,256]{1,0:T(8,128)} copy(f32[256,256]{0,1:T(8,128)} %reduce-scatter.2.cloned.1.call-done) | data formatting | bytes 524288
  (23 shorter events, 0.2 us)
Async XLA Ops:
  7.2 33.6 %copy-start.4 = (bf16[128,256]{1,0:T(8,128)(2,1)S(1)}, bf16[128,256]{1,0:T(8,128)(2,1)}, u32[]{:S(2)}) copy-start(bf16[128,256]{1,0:T(8,128)(2,1)} %param.8) | copy-start | bytes 196612
  7.2 25.8 %copy-start.6 = (bf16[128,2048]{1,0:T(8,128)(2,1)S(1)}, bf16[128,2048]{1,0:T(8,128)(2,1)}, u32[]{:S(2)}) copy-start(bf16[128,2048]{1,0:T(8,128)(2,1)} %param.11) | copy-start | bytes 1572868
  8.7 13.8 %all-to-all-start = ((s32[16,1,1]{2,1,0:T(1,128)}), s32[16,1,1]{2,1,0:T(1,128)S(1)}, u32[]{:S(2)}, u32[]{:S(2)}) async-start(s32[16,1,1]{2,1,0:T(1,128)} %copy.55), calls=%async_computation | async-start | bytes 16384 | tf_op jit(solution)/shard_map/all_to_all | solution.py:30
  27.2 13.5 %all-to-all-start.1 = ((bf16[16,32,256]{2,1,0:T(8,128)(2,1)}), bf16[16,32,256]{2,1,0:T(8,128)(2,1)S(1)}, u32[]{:S(2)}, u32[]{:S(2)}) async-start(bf16[16,32,256]{2,1,0:T(8,128)(2,1)} %get-tuple-element.31), calls=%async_computation.1 | async-start | bytes 524288 | tf_op jit(solution)/shard_map/all_to_all | solution.py:42
  33.1 9.1 %copy-start.2 = (bf16[16,8,16,128]{3,2,1,0:T(8,128)(2,1)}, bf16[16,8,16,128]{3,2,1,0:T(8,128)(2,1)S(1)}, u32[]{:S(2)}) copy-start(bf16[16,8,16,128]{3,2,1,0:T(8,128)(2,1)S(1)} %copy.80) | copy-start | bytes 1572868
  42.2 2.0 %copy-start = (f32[2,2,512,64,8]{2,3,4,1,0:T(8,128)}, f32[2,2,512,64,8]{2,3,4,1,0:T(8,128)S(1)}, u32[]{:S(2)}) copy-start(f32[2,2,512,64,8]{2,3,4,1,0:T(8,128)S(1)} %fusion.20) | copy-start | bytes 12582916
  49.3 17.8 %all-to-all-start.4 = ((f32[16,32,256]{2,1,0:T(8,128)}), f32[16,32,256]{2,1,0:T(8,128)S(1)}, u32[]{:S(2)}, u32[]{:S(2)}) async-start(f32[16,32,256]{2,1,0:T(8,128)} %bitcast.30), calls=%async_computation.4 | async-start | bytes 1048576 | tf_op jit(solution)/shard_map/all_to_all | solution.py:98
  52.8 25.0 %all-gather.2.cloned.1.call-start = ((), (), s32[]{:S(2)}) async-start(), calls=%async_computation.6 | async-start | bytes 1572864 | tf_op jit(solution)/shard_map/all_gather | solution.py:116
  53.6 108.9 %reduce-scatter.2.cloned.1.call-start = ((), (), s32[]{:S(2)}) async-start(), calls=%async_computation.7 | async-start | bytes 4456448 | tf_op jit(solution)/shard_map/reduce_scatter | solution.py:117
  67.9 9.9 %copy-start.7 = (f32[128,256]{1,0:T(8,128)}, f32[128,256]{1,0:T(8,128)S(1)}, u32[]{:S(2)}) copy-start(f32[128,256]{1,0:T(8,128)S(1)} %reshape.138) | copy-start | bytes 393220
  67.9 29.4 %copy-start.5 = (bf16[128,256]{1,0:T(8,128)(2,1)S(1)}, bf16[128,256]{1,0:T(8,128)(2,1)}, u32[]{:S(2)}) copy-start(bf16[128,256]{1,0:T(8,128)(2,1)} %param.9) | copy-start | bytes 196612
  81.7 16.3 %copy-start.3 = (bf16[16,8,16,128]{3,2,1,0:T(8,128)(2,1)S(1)}, bf16[16,8,16,128]{3,2,1,0:T(8,128)(2,1)}, u32[]{:S(2)}) copy-start(bf16[16,8,16,128]{3,2,1,0:T(8,128)(2,1)} %copy-done.2) | copy-start | bytes 1572868
  98.1 3.9 %copy-start.1 = (f32[2,2,512,64,8]{2,3,4,1,0:T(8,128)S(1)}, f32[2,2,512,64,8]{2,3,4,1,0:T(8,128)}, u32[]{:S(2)}) copy-start(f32[2,2,512,64,8]{2,3,4,1,0:T(8,128)} %copy-done) | copy-start | bytes 12582916
  112.0 23.7 %all-to-all-start.3 = ((f32[16,32,256]{2,1,0:T(8,128)}), f32[16,32,256]{2,1,0:T(8,128)}, u32[]{:S(2)}, u32[]{:S(2)}) async-start(f32[16,32,256]{2,1,0:T(8,128)} %bitcast.81), calls=%async_computation.3 | async-start | bytes 1048576 | tf_op jit(solution)/shard_map/all_to_all | solution.py:97
Sparse Core Ops, SparseCore 0:
  55.2 22.5 all-gather.1
  81.9 80.5 reduce-scatter.1
where the time goes:
time: 172 us; the launch traced here: 171 us
  waiting for transfers between devices  78.9 us (46%)
  local copies, waits for them, and re-layouts  24.1 us (14%)
  starting transfers between devices  18.8 us (11%)
  blocking collectives  15.6 us (9%)
  matrix products  14.8 us (9%)
  between operations  14.4 us (8%)
  other arithmetic  4.43 us (3%)
    reduce_scatter x1, waiting for transfers between devices, local(): lax.psum_scatter(jnp.einsum('td,tc->dc', full_input, value_low, preferred...  24.2 us
    all_to_all x1, waiting for transfers between devices, local(): lax.all_to_all(back_keys, 'kv', split_axis=0, concat_axis=0, tiled=True)  17 us
    all_to_all x1, blocking collectives, local(): lax.all_to_all(send_values, 'kv', split_axis=0, concat_axis=0, tiled=True)  15.6 us
    all_to_all x1, waiting for transfers between devices, local(): lax.all_to_all(back_values, 'kv', split_axis=0, concat_axis=0, tiled=True)  13.5 us
    all_gather x1, waiting for transfers between devices, local(): full_input = lax.all_gather(normed_input, 'tp', axis=1, tiled=True)  9.91 us
    unnamed x23, local copies, waits for them, and re-layouts  8.89 us
    all_to_all x1, waiting for transfers between devices, local(): lax.all_to_all(send_keys, 'kv', split_axis=0, concat_axis=0, tiled=True)  7.44 us
    all_to_all x1, starting transfers between devices, local(): lax.all_to_all(wanted.reshape(devices, 1), 'kv', split_axis=0, concat_axi...  7.39 us
  transfers between devices with their start and end apart: 6, of which 6 were waited for; matrix products, arithmetic and copies ran while one was open for 13% of the time, Pallas kernels for 0%

commit v1 on v0

--- a/solution.py
+++ b/solution.py
@@ -113,7 +113,7 @@
     key_grad = key_grad.reshape(tok, kv_cols)
     value_grad = value_grad.reshape(tok, kv_cols)
     value_low = value_grad.astype(jnp.bfloat16)
-    full_input = lax.all_gather(normed_input, "tp", axis=1, tiled=True)
+    full_input = jnp.concatenate(lax.all_gather(normed_input, "tp"), axis=1)
     weight_grad = lax.psum_scatter(
         jnp.einsum("td,tc->dc", full_input, value_low, preferred_element_type=jnp.float32),
         "kv",

time: 172 us -> 162 us (0.942)
  waiting for transfers between devices: 78.9 us -> 68.4 us
  local copies, waits for them, and re-layouts: 24.1 us -> 26.4 us
    all_gather x1, waiting for transfers between devices: 9.91 us -> 0.02 us  [local(): full_input = jnp.concatenate(lax.all_gather(normed_input, 'tp'), axis=1)]
    unnamed x23 -> x27, local copies, waits for them, and re-layouts: 8.89 us -> 8.9 us
  transfers between devices with their start and end apart: 6 -> 6, of which waited for: 6 -> 5; matrix products, arithmetic and copies ran while one was open for 13% -> 23% of each run, Pallas kernels for 0% -> 0%
where the time goes in v1:
time: 162 us; the launch traced here: 161 us
  waiting for transfers between devices  68.4 us (42%)
  local copies, waits for them, and re-layouts  26.4 us (16%)
  starting transfers between devices  18.8 us (12%)
  between operations  14.4 us (9%)
  matrix products  14.3 us (9%)
  blocking collectives  14 us (9%)
  other arithmetic  4.37 us (3%)
    reduce_scatter x1, waiting for transfers between devices, local(): lax.psum_scatter(jnp.einsum('td,tc->dc', full_input, value_low, preferred...  24.4 us
    all_to_all x1, waiting for transfers between devices, local(): lax.all_to_all(back_keys, 'kv', split_axis=0, concat_axis=0, tiled=True)  17 us
    all_to_all x1, blocking collectives, local(): lax.all_to_all(send_values, 'kv', split_axis=0, concat_axis=0, tiled=True)  14 us
    all_to_all x1, waiting for transfers between devices, local(): lax.all_to_all(back_values, 'kv', split_axis=0, concat_axis=0, tiled=True)  12.5 us
    unnamed x27, local copies, waits for them, and re-layouts  8.9 us
    all_to_all x1, waiting for transfers between devices, local(): lax.all_to_all(send_keys, 'kv', split_axis=0, concat_axis=0, tiled=True)  7.43 us
    all_to_all x1, starting transfers between devices, local(): lax.all_to_all(wanted.reshape(devices, 1), 'kv', split_axis=0, concat_axi...  7.39 us
    all_to_all x1, waiting for transfers between devices, local(): lax.all_to_all(wanted.reshape(devices, 1), 'kv', split_axis=0, concat_axi...  6.27 us
  transfers between devices with their start and end apart: 6, of which 5 were waited for; matrix products, arithmetic and copies ran while one was open for 23% of the time, Pallas kernels for 0%

profile of v1, /device:TPU:0, one launch (start us, length us, event | category | flops | bytes accessed | tf_op | source)
XLA Modules:
  0.0 160.7 jit_solution(11871907945134451082)
XLA Ops:
  7.2 0.0 all-gather.3.cloned.1.call-start
  7.2 0.7 all-gather.3.cloned.1.call-update
  7.9 0.7 compare_select_fusion
  8.6 0.1 select_reduce_fusion
  8.7 0.7 copy.70
  9.4 7.4 %all-to-all-start = ((s32[16,1,1]{2,1,0:T(1,128)}), s32[16,1,1]{2,1,0:T(1,128)S(1)}, u32[]{:S(2)}, u32[]{:S(2)}) async-start(s32[16,1,1]{2,1,0:T(1,128)} %copy.70), calls=%async_computation | async-start | bytes 16384 | tf_op jit(solution)/shard_map/all_to_all | solution.py:30
  16.8 0.1 reshape.158
  16.9 6.3 %all-to-all-done = s32[16,1,1]{2,1,0:T(1,128)S(1)} async-done(((s32[16,1,1]{2,1,0:T(1,128)}), s32[16,1,1]{2,1,0:T(1,128)S(1)}, u32[]{:S(2)}, u32[]{:S(2)}) %all-to-all-start) | async-done | bytes 96 | tf_op jit(solution)/shard_map/all_to_all | solution.py:30
  23.2 0.7 fusion.34
  23.8 1.4 gather_fusion.2
  25.3 1.4 gather_fusion
  26.7 0.4 compare_reduce_fusion
  27.1 0.8 broadcast_select_fusion.1
  27.9 3.5 %all-to-all-start.1 = ((bf16[16,32,256]{2,1,0:T(8,128)(2,1)}), bf16[16,32,256]{2,1,0:T(8,128)(2,1)S(1)}, u32[]{:S(2)}, u32[]{:S(2)}) async-start(bf16[16,32,256]{2,1,0:T(8,128)(2,1)} %get-tuple-element.35), calls=%async_computation.1 | async-start | bytes 524288 | tf_op jit(solution)/shard_map/all_to_all | solution.py:42
  31.4 0.1 eq.46
  31.5 0.1 add.89
  31.6 0.1 add.86
  31.7 0.1 add.87
  31.8 0.8 sub.31
  32.5 1.1 copy.95
  33.7 0.1 copy.96
  33.8 0.0 copy-start.4
  33.9 0.1 broadcast_compare_fusion
  34.0 7.4 %all-to-all-done.1 = bf16[16,32,256]{2,1,0:T(8,128)(2,1)S(1)} async-done(((bf16[16,32,256]{2,1,0:T(8,128)(2,1)}), bf16[16,32,256]{2,1,0:T(8,128)(2,1)S(1)}, u32[]{:S(2)}, u32[]{:S(2)}) %all-to-all-start.1) | async-done | bytes 262176 | tf_op jit(solution)/shard_map/all_to_all | solution.py:42
  41.4 0.6 gather_fusion.1
  42.0 0.1 reshape.129
  42.2 0.7 fusion.20
  42.9 1.9 %copy-done = f32[2,2,512,64,8]{2,3,4,1,0:T(8,128)} copy-done((f32[2,2,512,64,8]{2,3,4,1,0:T(8,128)}, f32[2,2,512,64,8]{2,3,4,1,0:T(8,128)S(1)}, u32[]{:S(2)}) %copy-start) | copy-done | bytes 4194328
  44.8 1.8 %fusion.14 = f32[2,512,2,128]{3,1,2,0:T(8,128)S(1)} fusion(f32[2,2,512,64,8]{2,3,4,1,0:T(8,128)S(1)} %fusion.20, f32[2,64,2,8]{1,3,2,0:T(8,128)S(1)} %copy.73, pred[2,64,512]{2,1,0:T(8,128)(4,1)S(1)} %broadcast_compare_fusion, bf16[2,64,2,8,128]{4,3,2,1,0:T(8,128)(2,1)S(1)} %bitcast.83), kind=kOutput, calls=%fused_computation.24 | convolution fusion | flops 272629760 | bytes 5840896 | tf_op jit(solution)/shard_map/bqngj,bqngd->bjnd/dot_general | solution.py:76
  46.6 0.8 copy.81
  47.4 0.8 reshape.142
  48.3 0.6 fusion.27
  49.0 1.0 copy.99
  49.9 3.6 %all-to-all-start.4 = ((f32[16,32,256]{2,1,0:T(8,128)}), f32[16,32,256]{2,1,0:T(8,128)S(1)}, u32[]{:S(2)}, u32[]{:S(2)}) async-start(f32[16,32,256]{2,1,0:T(8,128)} %bitcast.34), calls=%async_computation.4 | async-start | bytes 1048576 | tf_op jit(solution)/shard_map/all_to_all | solution.py:98
  53.5 0.0 reduce-scatter.2.cloned.1.call-start
  53.6 0.0 all-gather.3.cloned.1.call-done
  53.6 1.6 %copy.82 = bf16[128,2,2048]{0,2,1:T(8,128)(2,1)S(1)} copy(bf16[128,2,2048]{2,0,1:T(8,128)(2,1)} %bitcast.96) | data formatting | bytes 2097152 | tf_op jit(solution)/shard_map/reshape | solution.py:116
  55.2 12.5 %all-to-all-done.4 = f32[16,32,256]{2,1,0:T(8,128)S(1)} async-done(((f32[16,32,256]{2,1,0:T(8,128)}), f32[16,32,256]{2,1,0:T(8,128)S(1)}, u32[]{:S(2)}, u32[]{:S(2)}) %all-to-all-start.4) | async-done | bytes 524320 | tf_op jit(solution)/shard_map/all_to_all | solution.py:98
  67.8 0.3 copy.100
  68.1 1.0 fusion.37
  69.2 2.7 %convolution_bitcast_fusion = f32[4096,256]{0,1:T(8,128)} fusion(bf16[128,256]{1,0:T(8,128)(2,1)S(1)} %convert_element_type.17, bf16[128,4096]{0,1:T(8,128)(2,1)S(1)} %bitcast.80), kind=kOutput, calls=%fused_computation.6 | convolution fusion | flops 268435456 | bytes 5308416 | tf_op jit(solution)/shard_map/td,tc->dc/dot_general | solution.py:118
  71.9 0.0 reduce-scatter.2.cloned.1.call-update
  71.9 14.0 %all_to_all.29 = bf16[16,32,256]{2,1,0:T(8,128)(2,1)S(1)} all-to-all(bf16[16,32,256]{2,1,0:T(8,128)(2,1)S(1)} %get-tuple-element.36), channel_id=1, replica_groups=mesh['kv'=16,'tp'=2] {'kv'}, dimensions={0} | all-to-all | bytes 524288 | tf_op jit(solution)/shard_map/all_to_all | solution.py:43
  86.0 0.6 gather_fusion.3
  86.5 0.1 reshape.135
  86.7 3.6 %fusion = (f32[2,64,2,8]{1,3,2,0:T(8,128)S(1)}, f32[2,2,512,64,8]{2,3,4,1,0:T(8,128)S(1)}) fusion(f32[2,2,512,64,8]{2,3,4,1,0:T(8,128)} %copy-done, f32[2,64,2,8]{1,3,2,0:T(8,128)S(1)} %copy.73, pred[2,64,512]{2,1,0:T(8,128)(4,1)S(1)} %broadcast_compare_fusion, bf16[2,64,2,8,128]{4,3,2,1,0:T(8,128)(2,1)S(1)} %bitcast.84, ...), kind=kOutput, calls=%fused_computation.9 | convolution fusion | flops 273676288 | bytes 9519104 | tf_op jit(solution)/shard_map/bqngd,bjnd->bqngj/dot_general | solution.py:63
  90.3 0.3 copy-done.1
  90.6 1.5 fusion.2
  92.1 0.9 fusion.13
  93.0 1.8 %copy.79 = f32[2,512,2,128]{3,2,1,0:T(2,128)} copy(f32[2,512,2,128]{3,1,2,0:T(8,128)S(1)} %fusion.13) | data formatting | bytes 2097152 | tf_op jit(solution)/shard_map/mul | solution.py:73
  94.8 3.0 %reshape.138 = f32[32,8192]{1,0:T(8,128)} reshape(f32[2,512,2,128]{3,2,1,0:T(2,128)} %copy.79) | data formatting | bytes 2097152 | tf_op jit(solution)/shard_map/reshape | solution.py:84
  97.8 1.8 %fusion.28 = f32[20,8192]{1,0:T(8,128)S(1)} fusion(f32[32,8192]{1,0:T(8,128)} %reshape.138, s32[32]{0:T(128)S(1)} %eq.46), kind=kOutput, calls=%fused_computation.44 | convolution fusion | flops 62915200 | bytes 1704064 | tf_op jit(solution)/shard_map/dot_general | solution.py:82
  99.7 1.0 copy.97
  100.7 4.2 %all-to-all-start.3 = ((f32[16,32,256]{2,1,0:T(8,128)}), f32[16,32,256]{2,1,0:T(8,128)}, u32[]{:S(2)}, u32[]{:S(2)}) async-start(f32[16,32,256]{2,1,0:T(8,128)} %bitcast.88), calls=%async_computation.3 | async-start | bytes 1048576 | tf_op jit(solution)/shard_map/all_to_all | solution.py:97
  104.9 0.7 fusion.17
  105.7 0.6 copy.77
  106.3 1.1 reshape.137
  107.4 0.7 reshape.145
  108.2 17.0 %all-to-all-done.3 = f32[16,32,256]{2,1,0:T(8,128)} async-done(((f32[16,32,256]{2,1,0:T(8,128)}), f32[16,32,256]{2,1,0:T(8,128)}, u32[]{:S(2)}, u32[]{:S(2)}) %all-to-all-start.3) | async-done | bytes 524320 | tf_op jit(solution)/shard_map/all_to_all | solution.py:97
  125.2 1.4 copy.98
  126.6 0.4 convolution_add_fusion.1
  127.0 0.7 reshape.141
  127.7 24.4 %reduce-scatter.2.cloned.1.call-done = f32[256,256]{0,1:T(8,128)} async-done(((f32[4096,256]{0,1:T(8,128)}), f32[256,256]{0,1:T(8,128)}) %reduce-scatter.2.cloned.1.call-update) | async-done | bytes 262160 | tf_op jit(solution)/shard_map/reduce_scatter | solution.py:117
  152.1 1.8 %copy.83 = f32[256,256]{1,0:T(8,128)} copy(f32[256,256]{0,1:T(8,128)} %reduce-scatter.2.cloned.1.call-done) | data formatting | bytes 524288
  (29 shorter events, 0.3 us)
Async XLA Ops:
  7.2 34.2 %copy-start.6 = (bf16[128,256]{1,0:T(8,128)(2,1)S(1)}, bf16[128,256]{1,0:T(8,128)(2,1)}, u32[]{:S(2)}) copy-start(bf16[128,256]{1,0:T(8,128)(2,1)} %param.8) | copy-start | bytes 196612
  7.2 26.5 %copy-start.9 = (bf16[128,2048]{1,0:T(8,128)(2,1)S(1)}, bf16[128,2048]{1,0:T(8,128)(2,1)}, u32[]{:S(2)}) copy-start(bf16[128,2048]{1,0:T(8,128)(2,1)} %param.11) | copy-start | bytes 1572868
  7.2 46.4 %all-gather.3.cloned.1.call-start = ((), (), s32[]{:S(2)}) async-start(), calls=%async_computation.7 | async-start | bytes 1572864 | tf_op jit(solution)/shard_map/all_gather | solution.py:116
  9.4 13.8 %all-to-all-start = ((s32[16,1,1]{2,1,0:T(1,128)}), s32[16,1,1]{2,1,0:T(1,128)S(1)}, u32[]{:S(2)}, u32[]{:S(2)}) async-start(s32[16,1,1]{2,1,0:T(1,128)} %copy.70), calls=%async_computation | async-start | bytes 16384 | tf_op jit(solution)/shard_map/all_to_all | solution.py:30
  27.9 13.5 %all-to-all-start.1 = ((bf16[16,32,256]{2,1,0:T(8,128)(2,1)}), bf16[16,32,256]{2,1,0:T(8,128)(2,1)S(1)}, u32[]{:S(2)}, u32[]{:S(2)}) async-start(bf16[16,32,256]{2,1,0:T(8,128)(2,1)} %get-tuple-element.35), calls=%async_computation.1 | async-start | bytes 524288 | tf_op jit(solution)/shard_map/all_to_all | solution.py:42
  33.7 9.2 %copy-start.2 = (bf16[16,8,16,128]{3,2,1,0:T(8,128)(2,1)}, bf16[16,8,16,128]{3,2,1,0:T(8,128)(2,1)S(1)}, u32[]{:S(2)}) copy-start(bf16[16,8,16,128]{3,2,1,0:T(8,128)(2,1)S(1)} %copy.95) | copy-start | bytes 1572868
  33.8 9.1 %copy-start.4 = (bf16[16,8,16,128]{3,2,1,0:T(8,128)(2,1)}, bf16[16,8,16,128]{3,2,1,0:T(8,128)(2,1)S(1)}, u32[]{:S(2)}) copy-start(bf16[16,8,16,128]{3,2,1,0:T(8,128)(2,1)S(1)} %copy.96) | copy-start | bytes 1572868
  42.9 2.0 %copy-start = (f32[2,2,512,64,8]{2,3,4,1,0:T(8,128)}, f32[2,2,512,64,8]{2,3,4,1,0:T(8,128)S(1)}, u32[]{:S(2)}) copy-start(f32[2,2,512,64,8]{2,3,4,1,0:T(8,128)S(1)} %fusion.20) | copy-start | bytes 12582916
  49.9 17.8 %all-to-all-start.4 = ((f32[16,32,256]{2,1,0:T(8,128)}), f32[16,32,256]{2,1,0:T(8,128)S(1)}, u32[]{:S(2)}, u32[]{:S(2)}) async-start(f32[16,32,256]{2,1,0:T(8,128)} %bitcast.34), calls=%async_computation.4 | async-start | bytes 1048576 | tf_op jit(solution)/shard_map/all_to_all | solution.py:98
  53.5 98.6 %reduce-scatter.2.cloned.1.call-start = ((), (), s32[]{:S(2)}) async-start(), calls=%async_computation.6 | async-start | bytes 4456448 | tf_op jit(solution)/shard_map/reduce_scatter | solution.py:117
  69.1 16.8 %copy-start.7 = (bf16[128,256]{1,0:T(8,128)(2,1)S(1)}, bf16[128,256]{1,0:T(8,128)(2,1)}, u32[]{:S(2)}) copy-start(bf16[128,256]{1,0:T(8,128)(2,1)} %param.9) | copy-start | bytes 196612
  71.9 14.8 %copy-start.5 = (bf16[16,8,16,128]{3,2,1,0:T(8,128)(2,1)S(1)}, bf16[16,8,16,128]{3,2,1,0:T(8,128)(2,1)}, u32[]{:S(2)}) copy-start(bf16[16,8,16,128]{3,2,1,0:T(8,128)(2,1)} %copy-done.4) | copy-start | bytes 1572868
  86.7 3.9 %copy-start.1 = (f32[2,2,512,64,8]{2,3,4,1,0:T(8,128)S(1)}, f32[2,2,512,64,8]{2,3,4,1,0:T(8,128)}, u32[]{:S(2)}) copy-start(f32[2,2,512,64,8]{2,3,4,1,0:T(8,128)} %copy-done) | copy-start | bytes 12582916
  90.6 1.5 copy-start.3
  100.7 24.5 %all-to-all-start.3 = ((f32[16,32,256]{2,1,0:T(8,128)}), f32[16,32,256]{2,1,0:T(8,128)}, u32[]{:S(2)}, u32[]{:S(2)}) async-start(f32[16,32,256]{2,1,0:T(8,128)} %bitcast.88), calls=%async_computation.3 | async-start | bytes 1048576 | tf_op jit(solution)/shard_map/all_to_all | solution.py:97
  104.9 2.5 %copy-start.8 = (f32[4,8192]{1,0:T(4,128)S(1)}, f32[4,8192]{1,0:T(4,128)}, u32[]{:S(2)}) copy-start(f32[4,8192]{1,0:T(4,128)} %get-tuple-element.40) | copy-start | bytes 393220
Sparse Core Ops, SparseCore 0:
  9.5 23.9 all-gather.2
  72.0 80.0 reduce-scatter.1
